TPU v7x, 32 devices: a whole 2x2x4 slice. The times are simulated.
32 devices in a mesh: rep: 2 (over x), fs: 8 (over z, y), tp: 2 (over core).
Axes of the slice: x: 2, y: 2, z: 4, core: 2. Of those that a mesh axis runs over, the one named last changes fastest.
Arguments:
- input_activation_entries: bfloat16 [6144, 2048], P(('rep', 'fs')), may hold values from -6 to 6
- premixing_rescale_factor: float32 [2048], replicated, may hold values from 0.1 to 1.9
- probe_weight_table: float32 [2048, 1024], P('fs', 'tp'), may hold values from -0.125 to 0.125
- probe_factor_list: float32 [1024], P('tp'), may hold values from 0.5 to 2
- lookup_weight_table: float32 [2048, 1024], P('fs', 'tp'), may hold values from -0.125 to 0.125
- lookup_factor_list: float32 [1024], P('tp'), may hold values from 0.5 to 2
- forget_weight_table: float32 [2048, 1024], P('fs', 'tp'), may hold values from -0.125 to 0.125
- forget_factor_list: float32 [1024], P('tp'), may hold values from 1 to 8
- forget_shift_term: float32 [1024], P('tp'), may hold values from -3 to 7
- extra_forget_logs: float32 [6144, 8], P(('rep', 'fs'), 'tp'), may hold values from -0.7 to 0
- content_weight_table: float32 [2048, 2048], P('fs', 'tp'), may hold values from -0.125 to 0.125
- content_factor_list: float32 [2048], P('tp'), may hold values from 0.5 to 2
- filter_weight_table: float32 [2048, 2048], P('fs', 'tp'), may hold values from -0.125 to 0.125
- filter_factor_list: float32 [2048], P('tp'), may hold values from 0.5 to 2
- per_group_rescale_factor: float32 [2048], P('tp'), may hold values from 0.1 to 1.9
- emission_weight_table: float32 [2048, 2048], P('tp', 'fs'), may hold values from -0.125 to 0.125
- emission_factor_list: float32 [2048], P('fs'), may hold values from 0.5 to 2
- perceptron_prenorm_factor: float32 [2048], replicated, may hold values from 0.1 to 1.9
- raising_weight_table: float32 [2048, 8192], P('fs', 'tp'), may hold values from -0.125 to 0.125
- raising_factor_list: float32 [8192], P('tp'), may hold values from 0.5 to 2
- lowering_weight_table: float32 [8192, 2048], P('tp', 'fs'), may hold values from -0.0625 to 0.0625
- lowering_factor_list: float32 [2048], P('fs'), may hold values from 0.5 to 2
Outputs:
- layer_out: bfloat16 [6144, 2048], P(('rep', 'fs'))
All inputs are finite; a program needn't handle non-finite values.
Results may differ from a plain program's by a relative error of at most 0.02.
Values may be sent and summed in bfloat16 or wider, within the bound.
A program may use at most 128 MiB of HBM per device.

v0:
```python
import jax
import jax.numpy as jnp
from jax import lax
from jax.sharding import PartitionSpec as P

LOOKUP_FEATURES = 128
BLOCK = 64


epsilon = 1e-06
filter_rescaled_entries = 16.0
highest = lax.Precision.HIGHEST


def rms_rows(matrix, gain):
    matrix = matrix.astype(jnp.float32)
    return matrix * lax.rsqrt(jnp.mean(matrix * matrix, axis=-1, keepdims=True) + epsilon) * gain


def recur_head(queries, keys_in, vals, forget_log_rate):
    length = queries.shape[0]
    blocks = length // BLOCK

    def to_blocks(tensor):
        return tensor.astype(jnp.float32).reshape(blocks, BLOCK, tensor.shape[-1])

    causal = jnp.tril(jnp.ones((BLOCK, BLOCK), dtype=bool))[:, :, None]

    def advance(memory, inputs):
        query_block, key_block, value_block, decay_block = inputs
        cumulative = jnp.cumsum(decay_block, axis=0)
        spread = cumulative[:, None, :] - cumulative[None, :, :]
        weights = jnp.exp(jnp.where(causal, spread, -jnp.inf))
        scores = jnp.einsum("tc,sc,tsc->ts", query_block, key_block, weights, precision=highest)
        within = jnp.dot(scores, value_block, precision=highest)
        carried = jnp.dot(query_block * jnp.exp(cumulative), memory, precision=highest)
        closing = cumulative[-1]
        scaled_keys = key_block * jnp.exp(closing[None, :] - cumulative)
        memory = jnp.exp(closing)[:, None] * memory + jnp.dot(
            scaled_keys.T, value_block, precision=highest
        )
        return (memory, within + carried)

    initial = jnp.zeros((queries.shape[-1], vals.shape[-1]), jnp.float32)
    _, outputs = lax.scan(
        advance,
        initial,
        (to_blocks(queries), to_blocks(keys_in), to_blocks(vals), to_blocks(forget_log_rate)),
    )
    return outputs.reshape(length, vals.shape[-1])


def per_group_mixing_values(
    probe_mapped_entries,
    lookup_mapped_entries,
    forget_mapped_entries,
    content_mapped_entries,
    filter_mapped_entries,
    forget_shift_term,
    extra_forget_logs,
    per_group_rescale_factor,
):
    group_count_total = extra_forget_logs.shape[-1]
    queries = (jax.nn.silu(probe_mapped_entries) * LOOKUP_FEATURES ** (-0.5)).astype(jnp.bfloat16)
    keyed = jax.nn.silu(lookup_mapped_entries).astype(jnp.bfloat16)
    valued = jax.nn.silu(content_mapped_entries).astype(jnp.bfloat16)
    forget_log_rate = jax.nn.log_sigmoid(
        forget_mapped_entries + forget_shift_term
    ) / filter_rescaled_entries + jnp.repeat(extra_forget_logs, LOOKUP_FEATURES, axis=1)

    def by_head(tensor):
        return tensor.reshape(tensor.shape[0], group_count_total, -1).transpose(1, 0, 2)

    outputs = jax.vmap(recur_head)(
        by_head(queries), by_head(keyed), by_head(valued), by_head(forget_log_rate)
    )
    outputs = outputs * lax.rsqrt(jnp.mean(outputs * outputs, axis=-1, keepdims=True) + epsilon)
    merged = outputs.transpose(1, 0, 2).reshape(outputs.shape[1], -1)
    return (merged * per_group_rescale_factor * jax.nn.silu(filter_mapped_entries)).astype(
        jnp.bfloat16
    )


def body(
    input_activation_entries,
    premixing_rescale_factor,
    probe_weight_table,
    probe_factor_list,
    lookup_weight_table,
    lookup_factor_list,
    forget_weight_table,
    forget_factor_list,
    forget_shift_term,
    extra_forget_logs,
    content_weight_table,
    content_factor_list,
    filter_weight_table,
    filter_factor_list,
    per_group_rescale_factor,
    emission_weight_table,
    emission_factor_list,
    perceptron_prenorm_factor,
    raising_weight_table,
    raising_factor_list,
    lowering_weight_table,
    lowering_factor_list,
):
    whole_out_scale, whole_down_scale = (
        lax.all_gather(emission_factor_list, "fs", axis=0, tiled=True),
        lax.all_gather(lowering_factor_list, "fs", axis=0, tiled=True),
    )
    normed = rms_rows(input_activation_entries, premixing_rescale_factor).astype(jnp.bfloat16)
    query_bf = probe_weight_table.astype(jnp.bfloat16)
    key_bf = lookup_weight_table.astype(jnp.bfloat16)
    decay_bf = forget_weight_table.astype(jnp.bfloat16)
    value_bf = content_weight_table.astype(jnp.bfloat16)
    gate_bf = filter_weight_table.astype(jnp.bfloat16)
    out_bf = emission_weight_table.astype(jnp.bfloat16)
    up_bf = raising_weight_table.astype(jnp.bfloat16)
    down_bf = lowering_weight_table.astype(jnp.bfloat16)
    pieces = (
        lax.all_gather(query_bf, "fs", axis=0, tiled=True),
        lax.all_gather(key_bf, "fs", axis=0, tiled=True),
        lax.all_gather(decay_bf, "fs", axis=0, tiled=True),
        lax.all_gather(value_bf, "fs", axis=0, tiled=True),
        lax.all_gather(gate_bf, "fs", axis=0, tiled=True),
    )
    columns = normed
    projected = tuple(
        (
            jnp.dot(columns, shard_piece, preferred_element_type=jnp.float32)
            for shard_piece in pieces
        )
    )
    mixing_product = per_group_mixing_values(
        projected[0] * probe_factor_list,
        projected[1] * lookup_factor_list,
        projected[2] * forget_factor_list,
        projected[3] * content_factor_list,
        projected[4] * filter_factor_list,
        forget_shift_term,
        extra_forget_logs,
        per_group_rescale_factor,
    )
    column_scale = whole_out_scale
    mix_part = (
        jnp.dot(
            mixing_product,
            lax.all_gather(out_bf, "fs", axis=1, tiled=True),
            preferred_element_type=jnp.float32,
        )
        * column_scale
    )
    mix_rounded = lax.optimization_barrier(mix_part.astype(jnp.bfloat16)).astype(jnp.float32)
    mix_sum = lax.psum(mix_rounded.astype(jnp.bfloat16), "tp").astype(jnp.float32)
    residual = (input_activation_entries.astype(jnp.float32) + mix_sum).astype(jnp.bfloat16)
    normed_mlp = rms_rows(residual, perceptron_prenorm_factor).astype(jnp.bfloat16)
    columns = normed_mlp
    lifted = jnp.dot(
        columns, lax.all_gather(up_bf, "fs", axis=0, tiled=True), preferred_element_type=jnp.float32
    )
    hidden = jnp.square(jax.nn.relu(lifted * raising_factor_list)).astype(jnp.bfloat16)
    column_scale = whole_down_scale
    mlp_part = (
        jnp.dot(
            hidden,
            lax.all_gather(down_bf, "fs", axis=1, tiled=True),
            preferred_element_type=jnp.float32,
        )
        * column_scale
    )
    mlp_rounded = lax.optimization_barrier(mlp_part.astype(jnp.bfloat16)).astype(jnp.float32)
    mlp_sum = lax.psum(mlp_rounded.astype(jnp.bfloat16), "tp").astype(jnp.float32)
    return (residual.astype(jnp.float32) + mlp_sum).astype(jnp.bfloat16)


def solution(mesh):
    return jax.shard_map(
        body,
        mesh=mesh,
        in_specs=(
            P(("rep", "fs"), None),
            P(),
            P("fs", "tp"),
            P("tp"),
            P("fs", "tp"),
            P("tp"),
            P("fs", "tp"),
            P("tp"),
            P("tp"),
            P(("rep", "fs"), "tp"),
            P("fs", "tp"),
            P("tp"),
            P("fs", "tp"),
            P("tp"),
            P("tp"),
            P("tp", "fs"),
            P("fs"),
            P(),
            P("fs", "tp"),
            P("tp"),
            P("tp", "fs"),
            P("fs"),
        ),
        out_specs=P(("rep", "fs"), None),
        check_vma=False,
    )
```

profile of v0, /device:TPU:0, one launch (start us, length us, event | category | flops | bytes accessed | tf_op | source)
XLA Modules:
  0.0 922.1 jit_solution(15787063204989332477)
XLA Ops:
  13.3 2.1 convert_element_type.113
  16.0 22.3 %all-gather = f32[8,1,256]{2,1,0:T(1,128)S(1)} all-gather(f32[1,1,256]{2,1,0:T(1,128)S(1)} %bitcast.143), channel_id=1, replica_groups=mesh['rep'=2,'fs'=8,'tp'=2] {'fs'}, dimensions={0}, use_global_device_ids=true | all-gather | bytes 9216 | tf_op jit(solution)/shard_map/all_gather | solution.py:109
  38.3 23.2 %all-gather.11.cloned.1.call-done = bf16[2048,512]{1,0:T(8,128)(2,1)} async-done(((bf16[256,512]{1,0:T(8,128)(2,1)}), bf16[2048,512]{1,0:T(8,128)(2,1)}) %all-gather.11.cloned.1.call-update) | async-done | bytes 2097168 | tf_op jit(solution)/shard_map/all_gather | solution.py:124
  62.0 3.1 fusion.48
  66.1 45.2 %all-gather.17.cloned.1.call-done = bf16[2048,512]{1,0:T(8,128)(2,1)} async-done(((bf16[256,512]{1,0:T(8,128)(2,1)}), bf16[2048,512]{1,0:T(8,128)(2,1)}) %all-gather.17.cloned.1.call-update) | async-done | bytes 2097168 | tf_op jit(solution)/shard_map/all_gather | solution.py:122
  111.3 2.7 convert_bitcast_fusion
  115.0 46.1 %all-gather.13.cloned.1.call-done = bf16[2048,512]{1,0:T(8,128)(2,1)} async-done(((bf16[256,512]{1,0:T(8,128)(2,1)}), bf16[2048,512]{1,0:T(8,128)(2,1)}) %all-gather.13.cloned.1.call-update) | async-done | bytes 2097168 | tf_op jit(solution)/shard_map/all_gather | solution.py:123
  161.1 2.7 convert_bitcast_fusion.1
  163.9 70.5 %all-gather.15.cloned.1.call-done = bf16[2048,1024]{1,0:T(8,128)(2,1)} async-done(((bf16[256,1024]{1,0:T(8,128)(2,1)}), bf16[2048,1024]{1,0:T(8,128)(2,1)}) %all-gather.15.cloned.1.call-update) | async-done | bytes 4194320 | tf_op jit(solution)/shard_map/all_gather | solution.py:125
  234.4 4.2 fusion.42
  240.0 91.4 %while.13 = (s32[]{:T(128)}, f32[4,128,256]{2,1,0:T(8,128)S(1)}, f32[6,4,64,256]{3,2,0,1:T(8,128)}, f32[6,4,64,128]{3,2,0,1:T(8,128)}, f32[6,4,64,128]{3,2,0,1:T...) while((s32[]{:T(128)}, f32[4,128,256]{2,1,0:T(8,128)S(1)}, ...), condition=%wide.region_3.4_spmd.clone, body=%wide.region_1.3_spmd.clone.sunk | while | flops 264884224 | bytes 21781116 | solution.py:45
  242.7 7.4 fusion.81
  251.5 2.1 fusion.83
  257.9 7.4 fusion.81
  266.7 2.1 fusion.83
  273.2 7.4 fusion.81
  282.0 2.1 fusion.83
  288.4 7.4 fusion.81
  303.6 7.4 fusion.81
  318.9 7.4 fusion.81
  327.7 2.1 fusion.83
  333.9 49.0 %all-gather.21.cloned.1.call-done = bf16[1024,2048]{1,0:T(8,128)(2,1)} async-done(((bf16[1024,256]{1,0:T(8,128)(2,1)}), bf16[1024,2048]{1,0:T(8,128)(2,1)}) %all-gather.21.cloned.1.call-update) | async-done | bytes 4194320 | tf_op jit(solution)/shard_map/all_gather | solution.py:149
  382.9 8.3 multiply_convert_fusion.2
  391.3 3.8 convert_element_type.119
  395.1 3.9 convert_element_type.121
  399.6 18.2 %all-gather.1 = f32[8,1,256]{2,1,0:T(1,128)S(1)} all-gather(f32[1,1,256]{2,1,0:T(1,128)S(1)} %bitcast.144), channel_id=1, replica_groups=mesh['rep'=2,'fs'=8,'tp'=2] {'fs'}, dimensions={0}, use_global_device_ids=true | all-gather | bytes 9216 | tf_op jit(solution)/shard_map/all_gather | solution.py:110
  417.9 2.1 fusion.29
  420.0 220.5 %all-gather.23.cloned.1.call-done = bf16[2048,4096]{1,0:T(8,128)(2,1)} async-done(((bf16[256,4096]{1,0:T(8,128)(2,1)}), bf16[2048,4096]{1,0:T(8,128)(2,1)}) %all-gather.23.cloned.1.call-update) | async-done | bytes 16777232 | tf_op jit(solution)/shard_map/all_gather | solution.py:160
  640.6 227.6 %all-gather.25.cloned.1.call-done = bf16[4096,2048]{1,0:T(8,128)(2,1)} async-done(((bf16[4096,256]{1,0:T(8,128)(2,1)}), bf16[4096,2048]{1,0:T(8,128)(2,1)}) %all-gather.25.cloned.1.call-update) | async-done | bytes 16777232 | tf_op jit(solution)/shard_map/all_gather | solution.py:167
  868.1 25.0 %multiply_convert_fusion.1 = bf16[384,2048]{1,0:T(8,128)(2,1)} fusion(bf16[4096,2048]{1,0:T(8,128)(2,1)} %all-gather.25.cloned.1.call-done, bf16[2048,4096]{1,0:T(8,128)(2,1)} %all-gather.23.cloned.1.call-done, f32[4096]{0:T(1024)S(1)} %copy-done.9, f32[2048]{0:T(1024)S(1)} %bitcast.142, f32[2048]{0:T(1024)S(1)} %copy-done.11, f32[384]{0:T(512)S(1)} %add_rsqrt_fusion.1, ...), kind=kOutput, calls=%fused_computation.49 | convolution fusion | flops 12899057664 | bytes 38307328 | tf_op jit(solution)/shard_map/dot_general | solution.py:165
  893.1 18.7 %all-reduce.5.cloned.1.call-done = bf16[384,2048]{1,0:T(8,128)(2,1)} async-done(((bf16[384,2048]{1,0:T(8,128)(2,1)}), bf16[384,2048]{1,0:T(8,128)(2,1)}) %all-reduce.5.cloned.1.call-update) | async-done | bytes 1572880 | tf_op jit(solution)/shard_map/psum | solution.py:173
  911.8 3.4 fusion.32
  (137 shorter events, 52.6 us)
Async XLA Ops:
  6.5 3.9 copy-start.5
  6.5 4.7 copy-start.3
  6.5 55.0 %all-gather.11.cloned.1.call-start = ((), (), s32[]{:S(2)}) async-start(), calls=%async_computation | async-start | bytes 2359296 | tf_op jit(solution)/shard_map/all_gather | solution.py:124
  8.5 3.8 copy-start.4
  8.5 102.8 %all-gather.17.cloned.1.call-start = ((), (), s32[]{:S(2)}) async-start(), calls=%async_computation.3 | async-start | bytes 2359296 | tf_op jit(solution)/shard_map/all_gather | solution.py:122
  10.4 150.7 %all-gather.13.cloned.1.call-start = ((), (), s32[]{:S(2)}) async-start(), calls=%async_computation.1 | async-start | bytes 2359296 | tf_op jit(solution)/shard_map/all_gather | solution.py:123
  11.2 223.2 %all-gather.15.cloned.1.call-start = ((), (), s32[]{:S(2)}) async-start(), calls=%async_computation.2 | async-start | bytes 4718592 | tf_op jit(solution)/shard_map/all_gather | solution.py:125
  12.2 3.2 copy-start
  12.2 321.7 %all-gather.19.cloned.1.call-start = ((), (), s32[]{:S(2)}) async-start(), calls=%async_computation.4 | async-start | bytes 4718592 | tf_op jit(solution)/shard_map/all_gather | solution.py:126
  13.2 2.7 copy-start.6
  13.2 2.8 copy-start.7
  13.2 48.8 %copy-start.10 = (f32[2048]{0:T(1024)S(1)}, f32[2048]{0:T(1024)}, u32[]{:S(2)}) copy-start(f32[2048]{0:T(1024)} %param.25) | copy-start | bytes 24580
  13.2 48.8 %copy-start.15 = (f32[512]{0:T(512)S(1)}, f32[512]{0:T(512)}, u32[]{:S(2)}) copy-start(f32[512]{0:T(512)} %param.32) | copy-start | bytes 6148
  13.2 48.8 %copy-start.16 = (f32[512]{0:T(512)S(1)}, f32[512]{0:T(512)}, u32[]{:S(2)}) copy-start(f32[512]{0:T(512)} %param.31) | copy-start | bytes 6148
  13.2 369.6 %all-gather.21.cloned.1.call-start = ((), (), s32[]{:S(2)}) async-start(), calls=%async_computation.5 | async-start | bytes 4718592 | tf_op jit(solution)/shard_map/all_gather | solution.py:149
  15.4 402.5 %all-reduce.3.cloned.1.call-start = ((), (), s32[]{:S(2)}) async-start(), calls=%async_computation.6 | async-start | bytes 3145728 | tf_op jit(solution)/shard_map/psum | solution.py:155
  62.0 49.3 %copy-start.17 = (f32[512]{0:T(512)S(1)}, f32[512]{0:T(512)}, u32[]{:S(2)}) copy-start(f32[512]{0:T(512)} %param.27) | copy-start | bytes 6148
  66.1 95.0 %copy-start.18 = (f32[512]{0:T(512)S(1)}, f32[512]{0:T(512)}, u32[]{:S(2)}) copy-start(f32[512]{0:T(512)} %param.29) | copy-start | bytes 6148
  115.0 119.4 %copy-start.12 = (f32[1024]{0:T(1024)S(1)}, f32[1024]{0:T(1024)}, u32[]{:S(2)}) copy-start(f32[1024]{0:T(1024)} %param.35) | copy-start | bytes 12292
  331.4 1.9 copy-start.1
  333.6 49.2 %copy-start.13 = (f32[1024]{0:T(1024)S(1)}, f32[1024]{0:T(1024)}, u32[]{:S(2)}) copy-start(f32[1024]{0:T(1024)} %param.37) | copy-start | bytes 12292
  333.6 49.2 %copy-start.14 = (f32[1024]{0:T(1024)S(1)}, f32[1024]{0:T(1024)}, u32[]{:S(2)}) copy-start(f32[1024]{0:T(1024)} %param.38) | copy-start | bytes 12292
  391.2 249.3 %all-gather.23.cloned.1.call-start = ((), (), s32[]{:S(2)}) async-start(), calls=%async_computation.7 | async-start | bytes 18874368 | tf_op jit(solution)/shard_map/all_gather | solution.py:160
  395.1 473.1 %all-gather.25.cloned.1.call-start = ((), (), s32[]{:S(2)}) async-start(), calls=%async_computation.8 | async-start | bytes 18874368 | tf_op jit(solution)/shard_map/all_gather | solution.py:167
  399.0 0.7 copy-start.8
  399.0 469.1 %copy-start.9 = (f32[4096]{0:T(1024)S(1)}, f32[4096]{0:T(1024)}, u32[]{:S(2)}) copy-start(f32[4096]{0:T(1024)} %param.43) | copy-start | bytes 49156
  399.0 469.1 %copy-start.11 = (f32[2048]{0:T(1024)S(1)}, f32[2048]{0:T(1024)}, u32[]{:S(2)}) copy-start(f32[2048]{0:T(1024)} %param.41) | copy-start | bytes 24580
  399.0 512.8 %all-reduce.5.cloned.1.call-start = ((), (), s32[]{:S(2)}) async-start(), calls=%async_computation.9 | async-start | bytes 3145728 | tf_op jit(solution)/shard_map/psum | solution.py:173
  417.9 450.2 %copy-start.2 = (bf16[384,2048]{1,0:T(8,128)(2,1)S(1)}, bf16[384,2048]{1,0:T(8,128)(2,1)}, u32[]{:S(2)}) copy-start(bf16[384,2048]{1,0:T(8,128)(2,1)} %all-reduce.3.cloned.1.call-done) | copy-start | bytes 4718596
Sparse Core Ops, SparseCore 0:
  9.5 52.0 all-gather.10
  63.7 47.6 all-gather.16
  113.4 47.6 all-gather.12
  163.1 71.3 all-gather.14
  236.4 71.3 all-gather.18
  309.7 73.1 all-gather.20
  391.3 18.5 all-reduce.2
  412.1 228.4 all-gather.22
  642.6 225.4 all-gather.24
  893.3 18.5 all-reduce.4
where the time goes:
time: 923 us; the launch traced here: 922 us
  waiting for transfers between devices  701 us (76%)
  other arithmetic  78.2 us (8%)
  matrix products  76.7 us (8%)
  blocking collectives  40.6 us (4%)
  between operations  13.8 us (1%)
  local copies, waits for them, and re-layouts  11 us (1%)
    all_gather x1, waiting for transfers between devices, body(): lax.all_gather(down_bf, 'fs', axis=1, tiled=True)  228 us
    all_gather x1, waiting for transfers between devices, body(): lax.all_gather(up_bf, 'fs', axis=0, tiled=True)  221 us
    all_gather x1, waiting for transfers between devices, body(): lax.all_gather(value_bf, 'fs', axis=0, tiled=True)  70.5 us
    all_gather x1, waiting for transfers between devices, body(): lax.all_gather(out_bf, 'fs', axis=1, tiled=True)  49 us
    all_gather x1, waiting for transfers between devices, body(): lax.all_gather(key_bf, 'fs', axis=0, tiled=True)  46.1 us
    all_gather x1, waiting for transfers between devices, body(): lax.all_gather(query_bf, 'fs', axis=0, tiled=True)  45.2 us
    dot_general x6, other arithmetic, advance(): jnp.einsum('tc,sc,tsc->ts', query_block, key_block, weights, precision=hi...  44.3 us
    dot_general x1, matrix products, body(): jnp.dot(hidden, lax.all_gather(down_bf, 'fs', axis=1, tiled=True), prefer...  25 us
  transfers between devices with their start and end apart: 10, of which 8 were waited for; matrix products, arithmetic and copies ran while one was open for 14% of the time, Pallas kernels for 0%

commit v1 on v0

--- a/solution.py
+++ b/solution.py
@@ -1,10 +1,11 @@
 import jax
 import jax.numpy as jnp
 from jax import lax
-from jax.sharding import PartitionSpec as P
+from jax.sharding import Mesh, PartitionSpec as P
 
 LOOKUP_FEATURES = 128
 BLOCK = 64
+GROUP = 4
 
 
 epsilon = 1e-06
@@ -81,7 +82,7 @@
     )
 
 
-def body(
+def plain_body(
     input_activation_entries,
     premixing_rescale_factor,
     probe_weight_table,
@@ -174,34 +175,188 @@
     return (residual.astype(jnp.float32) + mlp_sum).astype(jnp.bfloat16)
 
 
+def swap(value, axis):
+    return lax.ppermute(value, axis, [(0, 1), (1, 0)])
+
+
+def in_order(first, mine, theirs):
+    return jnp.stack([jnp.where(first, mine, theirs), jnp.where(first, theirs, mine)])
+
+
+def scaled_dot(rows, weight):
+    return jnp.dot(rows, weight, preferred_element_type=jnp.float32)
+
+
+def paired_body(
+    input_activation_entries,
+    premixing_rescale_factor,
+    probe_weight_table,
+    probe_factor_list,
+    lookup_weight_table,
+    lookup_factor_list,
+    forget_weight_table,
+    forget_factor_list,
+    forget_shift_term,
+    extra_forget_logs,
+    content_weight_table,
+    content_factor_list,
+    filter_weight_table,
+    filter_factor_list,
+    per_group_rescale_factor,
+    emission_weight_table,
+    emission_factor_list,
+    perceptron_prenorm_factor,
+    raising_weight_table,
+    raising_factor_list,
+    lowering_weight_table,
+    lowering_factor_list,
+):
+    side = lax.axis_index("y")
+    mine = 2 * lax.axis_index("rep") + side
+    core = lax.axis_index("tp")
+    first_core = core == 0
+    tokens, width = input_activation_entries.shape
+    half = tokens // 2
+
+    def share(tensor, axis, who=mine):
+        extent = tensor.shape[axis] // GROUP
+        return lax.dynamic_slice_in_dim(tensor, who * extent, extent, axis)
+
+    def across(value, distance):
+        return lax.ppermute(value, ("rep", "y"), [(i, i ^ distance) for i in range(GROUP)])
+
+    def shared(rows):
+        pieces = jnp.stack([rows] + [across(rows, d) for d in range(1, GROUP)])
+        pieces = in_order(first_core, pieces, swap(pieces, "tp"))
+        return pieces.transpose(1, 0, 2, 3).reshape(GROUP * tokens, width)
+
+    def half_rows(tensor, who=core):
+        return lax.dynamic_slice_in_dim(tensor, who * half, half, tensor.ndim - 2)
+
+    scales = lax.all_gather(
+        jnp.stack([emission_factor_list, lowering_factor_list]), ("z", "y"), axis=1, tiled=True
+    )
+    def gathered(tables, cut, joined, along):
+        def piece(who):
+            shares = [share(table, cut, who).astype(jnp.bfloat16) for table in tables]
+            return jnp.concatenate(shares, axis=joined)
+
+        pair = in_order(side == 0, piece(mine), swap(piece(mine ^ 1), "y"))
+        pair = jnp.concatenate([pair[0], pair[1]], axis=along)
+        return lax.all_gather(pair, "z", axis=along, tiled=True)
+
+    entry_whole = gathered(
+        (
+            probe_weight_table,
+            lookup_weight_table,
+            forget_weight_table,
+            content_weight_table,
+            filter_weight_table,
+        ),
+        1,
+        1,
+        0,
+    )
+    exits_whole = gathered((emission_weight_table, lowering_weight_table), 0, 0, 1)
+    out_rows = emission_weight_table.shape[0] // GROUP
+    out_whole, down_whole = exits_whole[:out_rows], exits_whole[out_rows:]
+    up_whole = gathered((raising_weight_table,), 1, 1, 0)
+
+    normed = rms_rows(input_activation_entries, premixing_rescale_factor).astype(jnp.bfloat16)
+    both = shared(half_rows(normed))
+    bursts = jnp.stack(
+        [share(extra_forget_logs, 1)]
+        + [across(share(extra_forget_logs, 1, mine ^ d), d) for d in range(1, GROUP)]
+    )
+
+    factors = [
+        share(factor, 0)
+        for factor in (
+            probe_factor_list,
+            lookup_factor_list,
+            forget_factor_list,
+            content_factor_list,
+            filter_factor_list,
+        )
+    ]
+    projected = scaled_dot(both, entry_whole) * jnp.concatenate(factors)
+    pieces, start = [], 0
+    for factor in factors:
+        stop = start + factor.shape[0]
+        pieces.append(projected[:, start:stop].reshape(GROUP, tokens, -1))
+        start = stop
+    shift, gain = share(forget_shift_term, 0), share(per_group_rescale_factor, 0)
+    mixing_product = jax.vmap(
+        lambda q, k, d, v, g, b: per_group_mixing_values(q, k, d, v, g, shift, b, gain)
+    )(*pieces, bursts)
+
+    def summed(product, weight, scale):
+        part = (scaled_dot(product, weight) * scale).astype(jnp.bfloat16).reshape(GROUP, tokens, width)
+        theirs = swap(half_rows(part, 1 - core), "tp")
+        total = half_rows(part).astype(jnp.float32) + theirs.astype(jnp.float32)
+        outgoing = total.astype(jnp.bfloat16)
+        result = total[0]
+        for d in range(1, GROUP):
+            result = result + across(outgoing[d], d).astype(jnp.float32)
+        return result
+
+    mix_sum = summed(mixing_product.reshape(GROUP * tokens, -1), out_whole, scales[0])
+    entries = half_rows(input_activation_entries)
+    residual = (entries.astype(jnp.float32) + mix_sum).astype(jnp.bfloat16)
+    normed_mlp = rms_rows(residual, perceptron_prenorm_factor).astype(jnp.bfloat16)
+    columns = shared(normed_mlp)
+    lifted = scaled_dot(columns, up_whole) * share(raising_factor_list, 0)
+    hidden = jnp.square(jax.nn.relu(lifted)).astype(jnp.bfloat16)
+    mlp_sum = summed(hidden, down_whole, scales[1])
+    layer_half = (residual.astype(jnp.float32) + mlp_sum).astype(jnp.bfloat16)
+    return in_order(first_core, layer_half, swap(layer_half, "tp")).reshape(tokens, width)
+
+
+def specs_over(fs):
+    in_specs = (
+        P(("rep", *fs), None),
+        P(),
+        P(fs, "tp"),
+        P("tp"),
+        P(fs, "tp"),
+        P("tp"),
+        P(fs, "tp"),
+        P("tp"),
+        P("tp"),
+        P(("rep", *fs), "tp"),
+        P(fs, "tp"),
+        P("tp"),
+        P(fs, "tp"),
+        P("tp"),
+        P("tp"),
+        P("tp", fs),
+        P(fs),
+        P(),
+        P(fs, "tp"),
+        P("tp"),
+        P("tp", fs),
+        P(fs),
+    )
+    return in_specs, P(("rep", *fs), None)
+
+
 def solution(mesh):
-    return jax.shard_map(
-        body,
-        mesh=mesh,
-        in_specs=(
-            P(("rep", "fs"), None),
-            P(),
-            P("fs", "tp"),
-            P("tp"),
-            P("fs", "tp"),
-            P("tp"),
-            P("fs", "tp"),
-            P("tp"),
-            P("tp"),
-            P(("rep", "fs"), "tp"),
-            P("fs", "tp"),
-            P("tp"),
-            P("fs", "tp"),
-            P("tp"),
-            P("tp"),
-            P("tp", "fs"),
-            P("fs"),
-            P(),
-            P("fs", "tp"),
-            P("tp"),
-            P("tp", "fs"),
-            P("fs"),
-        ),
-        out_specs=P(("rep", "fs"), None),
-        check_vma=False,
-    )
+    sizes = mesh.shape
+    plain_in, plain_out = specs_over(("fs",))
+    plain = jax.shard_map(
+        plain_body, mesh=mesh, in_specs=plain_in, out_specs=plain_out, check_vma=False
+    )
+    if sizes["rep"] != 2 or sizes["tp"] != 2 or sizes["fs"] % 2:
+        return plain
+    split_mesh = Mesh(mesh.devices.reshape(2, sizes["fs"] // 2, 2, 2), ("rep", "z", "y", "tp"))
+    group_in, group_out = specs_over(("z", "y"))
+    grouped = jax.shard_map(
+        paired_body, mesh=split_mesh, in_specs=group_in, out_specs=group_out, check_vma=False
+    )
+
+    def layer(*arrays):
+        heads = arrays[9].shape[1] // sizes["tp"]
+        tokens = arrays[0].shape[0] // (sizes["rep"] * sizes["fs"])
+        return (plain if heads % GROUP or tokens % 32 else grouped)(*arrays)
+
+    return layer

time: 923 us -> 417 us (0.45)
  waiting for transfers between devices: 701 us -> 159 us
  local copies, waits for them, and re-layouts: 11 us -> 40.8 us
  matrix products: 76.7 us -> 52.3 us
  starting transfers between devices: 0.38 us -> 24.5 us
  other arithmetic: 78.2 us -> 89.8 us
    all_gather x8 -> x3, waiting for transfers between devices: 682 us -> 0.02 us  [gathered(): return lax.all_gather(pair, 'z', axis=along, tiled=True)]
    ppermute x0 -> x23, waiting for transfers between devices: none -> 158 us  [the longest x15 131 us: across(): lax.ppermute(value, ('rep', 'y'), [(i, i ^ distance) for i in range(GROUP)])]
    ppermute x0 -> x23, starting transfers between devices: none -> 24.5 us  [the longest x15 17.7 us: across(): lax.ppermute(value, ('rep', 'y'), [(i, i ^ distance) for i in range(GROUP)])]
    psum x2 -> x0, waiting for transfers between devices: 18.7 us -> none  [the longest x1 18.7 us: body(): lax.psum(mlp_rounded.astype(jnp.bfloat16), 'tp').astype(jnp.float32)]
    dot_general x6 -> x3, matrix products: 46.1 us -> 33.3 us  [scaled_dot(): return jnp.dot(rows, weight, preferred_element_type=jnp.float32)]
    another operation x0 -> x17, other arithmetic: none -> 10.5 us  [the longest x5 7.64 us: in_order(): jnp.stack([jnp.where(first, mine, theirs), jnp.where(first, theirs, mine)])]
    unnamed x39 -> x54, local copies, waits for them, and re-layouts: 0.81 us -> 11 us
    convert_element_type x9 -> x7, other arithmetic: 19.3 us -> 11.1 us  [the longest x2 6.18 us: summed(): outgoing = total.astype(jnp.bfloat16)]
  transfers between devices with their start and end apart: 10 -> 26, of which waited for: 8 -> 18; matrix products, arithmetic and copies ran while one was open for 14% -> 34% of each run, Pallas kernels for 0% -> 0%
where the time goes in v1:
time: 417 us; the launch traced here: 416 us
  waiting for transfers between devices  159 us (38%)
  other arithmetic  89.8 us (22%)
  matrix products  52.3 us (13%)
  local copies, waits for them, and re-layouts  40.8 us (10%)
  blocking collectives  36 us (9%)
  starting transfers between devices  24.5 us (6%)
  between operations  13.6 us (3%)
    ppermute x15, waiting for transfers between devices, across(): lax.ppermute(value, ('rep', 'y'), [(i, i ^ distance) for i in range(GROUP)])  131 us
    dot_general x6, other arithmetic, advance(): jnp.einsum('tc,sc,tsc->ts', query_block, key_block, weights, precision=hi...  44.3 us
    all_gather x1, blocking collectives, paired_body(): lax.all_gather(jnp.stack([emission_factor_list, lowering_factor_list]), (...  36 us
    dot_general x3, matrix products, scaled_dot(): return jnp.dot(rows, weight, preferred_element_type=jnp.float32)  33.3 us
    ppermute x8, waiting for transfers between devices, swap(): return lax.ppermute(value, axis, [(0, 1), (1, 0)])  27.7 us
    ppermute x15, starting transfers between devices, across(): lax.ppermute(value, ('rep', 'y'), [(i, i ^ distance) for i in range(GROUP)])  17.7 us
    dot_general x6, matrix products, advance(): jnp.dot(query_block * jnp.exp(cumulative), memory, precision=highest)  12.4 us
    unnamed x54, local copies, waits for them, and re-layouts  11 us
  transfers between devices with their start and end apart: 26, of which 18 were waited for; matrix products, arithmetic and copies ran while one was open for 34% of the time, Pallas kernels for 0%

profile of v1, /device:TPU:0, one launch (start us, length us, event | category | flops | bytes accessed | tf_op | source)
XLA Modules:
  0.0 416.1 jit_solution(18030955859314836826)
XLA Ops:
  11.7 3.1 collective-permute-start.4
  14.8 10.5 %collective-permute-done.4 = bf16[256,896]{1,0:T(8,128)(2,1)S(1)} collective-permute-done((bf16[256,896]{1,0:T(8,128)(2,1)S(1)}, bf16[256,896]{1,0:T(8,128)(2,1)S(1)}, u32[]{:S(2)}, u32[]{:S(2)}) %collective-permute-start.4) | collective-permute-done | bytes 458784 | tf_op jit(solution)/shard_map/ppermute | solution.py:179
  34.2 15.8 %collective-permute-done = bf16[192,2048]{1,0:T(8,128)(2,1)S(1)} collective-permute-done((bf16[192,2048]{1,0:T(8,128)(2,1)S(1)}, bf16[192,2048]{1,0:T(8,128)(2,1)S(1)}, u32[]{:S(2)}, u32[]{:S(2)}) %collective-permute-start) | collective-permute-done | bytes 786464 | tf_op jit(solution)/shard_map/ppermute | solution.py:226
  50.0 2.6 collective-permute-done.1
  52.6 14.6 %collective-permute-done.2 = bf16[192,2048]{1,0:T(8,128)(2,1)S(1)} collective-permute-done((bf16[192,2048]{1,0:T(8,128)(2,1)S(1)}, bf16[192,2048]{1,0:T(8,128)(2,1)S(1)}, u32[]{:S(2)}, u32[]{:S(2)}) %collective-permute-start.2) | collective-permute-done | bytes 786464 | tf_op jit(solution)/shard_map/ppermute | solution.py:226
  77.2 36.0 %all_gather.14 = f32[2,2048]{1,0:T(2,128)S(1)} all-gather(f32[2,256]{1,0:T(2,128)S(1)} %pad_maximum_fusion.10), channel_id=1, replica_groups=mesh['rep'=2,'z'=4,'y'=2,'tp'=2] {'z','y'}, dimensions={1}, use_global_device_ids=true | all-gather | bytes 18432 | tf_op jit(solution)/shard_map/all_gather | solution.py:236
  124.3 2.4 select_bitcast_fusion.3
  126.7 3.2 pad_maximum_fusion
  130.0 10.5 %convolution_multiply_fusion = f32[1536,896]{1,0:T(8,128)S(1)} fusion(bf16[1536,2048]{1,0:T(8,128)(2,1)} %bitcast.186, bf16[2048,896]{1,0:T(8,128)(2,1)} %all-gather.4.cloned.1.call-done, f32[896]{0:T(1024)S(1)} %copy-done.22), kind=kOutput, calls=%fused_computation.44 | convolution fusion | flops 5638520832 | bytes 15470080 | tf_op jit(solution)/shard_map/dot_general | solution.py:187
  145.4 85.0 %while.13 = (s32[]{:T(128)}, f32[4,1,128,256]{3,2,0,1:T(8,128)S(1)}, f32[6,4,1,64,256]{4,3,1,2,0:T(8,128)}, f32[6,4,1,64,128]{4,3,1,2,0:T(8,128)}, f32[6,4,1,64,...) while((s32[]{:T(128)}, ...), condition=%wide.region_3.4_spmd.clone, body=%wide.region_1.3_spmd.clone.sunk | while | flops 264884224 | bytes 21846144 | solution.py:46
  148.9 7.4 %fusion.94 = f32[4,64,64]{1,2,0:T(8,128)S(1)} fusion(f32[4,64,64,128]{3,2,1,0:T(8,128)S(1)} %select_exponential_fusion.2, f32[4,128,64]{1,2,0:T(8,128)S(1)} %get-tuple-element.184, f32[4,128,64]{1,2,0:T(8,128)S(1)} %get-tuple-element.185), kind=kLoop, calls=%fused_computation.2.clone.1 | loop fusion | flops 6275072 | bytes 8716288 | tf_op jit(solution)/shard_map/vmap(vmap())/while/body/eval_jaxpr/tc,sc,tsc->ts/dot_general | solution.py:35
  163.0 7.4 %fusion.94 = f32[4,64,64]{1,2,0:T(8,128)S(1)} fusion(f32[4,64,64,128]{3,2,1,0:T(8,128)S(1)} %select_exponential_fusion.2, f32[4,128,64]{1,2,0:T(8,128)S(1)} %get-tuple-element.184, f32[4,128,64]{1,2,0:T(8,128)S(1)} %get-tuple-element.185), kind=kLoop, calls=%fused_computation.2.clone.1 | loop fusion | flops 6275072 | bytes 8716288 | tf_op jit(solution)/shard_map/vmap(vmap())/while/body/eval_jaxpr/tc,sc,tsc->ts/dot_general | solution.py:35
  177.2 7.4 %fusion.94 = f32[4,64,64]{1,2,0:T(8,128)S(1)} fusion(f32[4,64,64,128]{3,2,1,0:T(8,128)S(1)} %select_exponential_fusion.2, f32[4,128,64]{1,2,0:T(8,128)S(1)} %get-tuple-element.184, f32[4,128,64]{1,2,0:T(8,128)S(1)} %get-tuple-element.185), kind=kLoop, calls=%fused_computation.2.clone.1 | loop fusion | flops 6275072 | bytes 8716288 | tf_op jit(solution)/shard_map/vmap(vmap())/while/body/eval_jaxpr/tc,sc,tsc->ts/dot_general | solution.py:35
  191.3 7.4 %fusion.94 = f32[4,64,64]{1,2,0:T(8,128)S(1)} fusion(f32[4,64,64,128]{3,2,1,0:T(8,128)S(1)} %select_exponential_fusion.2, f32[4,128,64]{1,2,0:T(8,128)S(1)} %get-tuple-element.184, f32[4,128,64]{1,2,0:T(8,128)S(1)} %get-tuple-element.185), kind=kLoop, calls=%fused_computation.2.clone.1 | loop fusion | flops 6275072 | bytes 8716288 | tf_op jit(solution)/shard_map/vmap(vmap())/while/body/eval_jaxpr/tc,sc,tsc->ts/dot_general | solution.py:35
  205.5 7.4 %fusion.94 = f32[4,64,64]{1,2,0:T(8,128)S(1)} fusion(f32[4,64,64,128]{3,2,1,0:T(8,128)S(1)} %select_exponential_fusion.2, f32[4,128,64]{1,2,0:T(8,128)S(1)} %get-tuple-element.184, f32[4,128,64]{1,2,0:T(8,128)S(1)} %get-tuple-element.185), kind=kLoop, calls=%fused_computation.2.clone.1 | loop fusion | flops 6275072 | bytes 8716288 | tf_op jit(solution)/shard_map/vmap(vmap())/while/body/eval_jaxpr/tc,sc,tsc->ts/dot_general | solution.py:35
  219.6 7.4 %fusion.94 = f32[4,64,64]{1,2,0:T(8,128)S(1)} fusion(f32[4,64,64,128]{3,2,1,0:T(8,128)S(1)} %select_exponential_fusion.2, f32[4,128,64]{1,2,0:T(8,128)S(1)} %get-tuple-element.184, f32[4,128,64]{1,2,0:T(8,128)S(1)} %get-tuple-element.185), kind=kLoop, calls=%fused_computation.2.clone.1 | loop fusion | flops 6275072 | bytes 8716288 | tf_op jit(solution)/shard_map/vmap(vmap())/while/body/eval_jaxpr/tc,sc,tsc->ts/dot_general | solution.py:35
  234.8 3.0 multiply_convert_fusion.1
  241.2 2.7 collective-permute-done.9
  243.8 4.4 %fusion.68 = (bf16[4,192,2048]{2,1,0:T(8,128)(2,1)S(1)}, f32[4,192,2048]{2,1,0:T(8,128)}) fusion(bf16[4,192,2048]{2,1,0:T(8,128)(2,1)S(1)} %collective-permute-done.9, bf16[4,384,2048]{2,1,0:T(8,128)(2,1)S(1)} %bitcast.190, s32[]{:T(128)S(6)} %select_n.148), kind=kLoop, calls=%fused_computation.159 | loop fusion | flops 6291456 | bytes 15728644 | tf_op jit(solution)/shard_map/convert_element_type | solution.py:297
  256.9 14.9 %collective-permute-done.10 = bf16[192,2048]{1,0:T(8,128)(2,1)S(1)} collective-permute-done((bf16[192,2048]{1,0:T(8,128)(2,1)}, bf16[192,2048]{1,0:T(8,128)(2,1)S(1)}, u32[]{:S(2)}, u32[]{:S(2)}) %collective-permute-start.10) | collective-permute-done | bytes 786464 | tf_op jit(solution)/shard_map/ppermute | solution.py:226
  272.0 15.7 %collective-permute-done.12 = bf16[192,2048]{1,0:T(8,128)(2,1)} collective-permute-done((bf16[192,2048]{1,0:T(8,128)(2,1)}, bf16[192,2048]{1,0:T(8,128)(2,1)}, u32[]{:S(2)}, u32[]{:S(2)}) %collective-permute-start.12) | collective-permute-done | bytes 786464 | tf_op jit(solution)/shard_map/ppermute | solution.py:226
  287.7 2.6 fusion.31
  294.4 15.8 %collective-permute-done.13 = bf16[192,2048]{1,0:T(8,128)(2,1)S(1)} collective-permute-done((bf16[192,2048]{1,0:T(8,128)(2,1)S(1)}, bf16[192,2048]{1,0:T(8,128)(2,1)S(1)}, u32[]{:S(2)}, u32[]{:S(2)}) %collective-permute-start.13) | collective-permute-done | bytes 786464 | tf_op jit(solution)/shard_map/ppermute | solution.py:226
  310.2 2.5 collective-permute-done.14
  312.7 14.4 %collective-permute-done.15 = bf16[192,2048]{1,0:T(8,128)(2,1)S(1)} collective-permute-done((bf16[192,2048]{1,0:T(8,128)(2,1)S(1)}, bf16[192,2048]{1,0:T(8,128)(2,1)S(1)}, u32[]{:S(2)}, u32[]{:S(2)}) %collective-permute-start.15) | collective-permute-done | bytes 786464 | tf_op jit(solution)/shard_map/ppermute | solution.py:226
  327.6 5.6 %collective-permute-done.16 = bf16[4,192,2048]{2,1,0:T(8,128)(2,1)S(1)} collective-permute-done((bf16[4,192,2048]{2,1,0:T(8,128)(2,1)S(1)}, bf16[4,192,2048]{2,1,0:T(8,128)(2,1)S(1)}, u32[]{:S(2)}, u32[]{:S(2)}) %collective-permute-start.16) | collective-permute-done | bytes 3145760 | tf_op jit(solution)/shard_map/ppermute | solution.py:179
  334.5 3.3 copy.87
  337.8 19.7 %multiply_convert_fusion = bf16[1536,2048]{1,0:T(8,128)(2,1)} fusion(f32[2048]{0:T(1024)S(1)} %bitcast.210, bf16[1280,2048]{1,0:T(8,128)(2,1)} %all-gather.6.cloned.1.call-done, bf16[1536,2048]{1,0:T(8,128)(2,1)} %bitcast.185, bf16[2048,1024]{1,0:T(8,128)(2,1)} %all-gather.8.cloned.1.call-done, f32[1024]{0:T(1024)S(1)} %dynamic-slice-done), kind=kOutput, calls=%fused_computation.37 | convolution fusion | flops 12897484800 | bytes 20983808 | tf_op jit(solution)/shard_map/dot_general | solution.py:187
  360.0 5.5 %collective-permute-done.18 = bf16[4,192,2048]{2,1,0:T(8,128)(2,1)S(1)} collective-permute-done((bf16[4,192,2048]{2,1,0:T(8,128)(2,1)S(1)}, bf16[4,192,2048]{2,1,0:T(8,128)(2,1)S(1)}, u32[]{:S(2)}, u32[]{:S(2)}) %collective-permute-start.18) | collective-permute-done | bytes 3145760 | tf_op jit(solution)/shard_map/ppermute | solution.py:179
  371.1 16.1 %collective-permute-done.19 = bf16[192,2048]{1,0:T(8,128)(2,1)S(1)} collective-permute-done((bf16[192,2048]{1,0:T(8,128)(2,1)S(1)}, bf16[192,2048]{1,0:T(8,128)(2,1)S(1)}, u32[]{:S(2)}, u32[]{:S(2)}) %collective-permute-start.19) | collective-permute-done | bytes 786464 | tf_op jit(solution)/shard_map/ppermute | solution.py:226
  387.2 2.4 collective-permute-done.20
  389.6 15.6 %collective-permute-done.21 = bf16[192,2048]{1,0:T(8,128)(2,1)S(1)} collective-permute-done((bf16[192,2048]{1,0:T(8,128)(2,1)S(1)}, bf16[192,2048]{1,0:T(8,128)(2,1)S(1)}, u32[]{:S(2)}, u32[]{:S(2)}) %collective-permute-start.21) | collective-permute-done | bytes 786464 | tf_op jit(solution)/shard_map/ppermute | solution.py:226
  (216 shorter events, 114.6 us)
Async XLA Ops:
  6.5 123.5 %all-gather.4.cloned.1.call-start = ((), (), s32[]{:S(2)}) async-start(), calls=%async_computation | async-start | bytes 4587520 | tf_op jit(solution)/shard_map/all_gather | solution.py:246
  11.7 13.6 %collective-permute-start.4 = (bf16[256,896]{1,0:T(8,128)(2,1)S(1)}, bf16[256,896]{1,0:T(8,128)(2,1)S(1)}, u32[]{:S(2)}, u32[]{:S(2)}) collective-permute-start(bf16[256,896]{1,0:T(8,128)(2,1)S(1)} %get-tuple-element.120), channel_id=1, source_target_pairs={{0,2},{2,0},{1,3},{3,1},{4,6},{6,4},{5,7},{7,5},{8,10},{10,8},{9,1... | collective-permute-start | bytes 1376264 | tf_op jit(solution)/shard_map/ppermute | solution.py:179
  26.4 208.4 %all-gather.6.cloned.1.call-start = ((), (), s32[]{:S(2)}) async-start(), calls=%async_computation.1 | async-start | bytes 6553600 | tf_op jit(solution)/shard_map/all_gather | solution.py:246
  30.4 19.6 %collective-permute-start = (bf16[192,2048]{1,0:T(8,128)(2,1)S(1)}, bf16[192,2048]{1,0:T(8,128)(2,1)S(1)}, u32[]{:S(2)}, u32[]{:S(2)}) collective-permute-start(bf16[192,2048]{1,0:T(8,128)(2,1)S(1)} %fusion.44), channel_id=1, source_target_pairs={{0,2},{2,0},{16,18},{18,16},{1,3},{3,1},{17,19},{19,17},{4,6},{6,4... | collective-permute-start | bytes 2359304 | tf_op jit(solution)/shard_map/ppermute | solution.py:226
  32.2 20.4 %collective-permute-start.1 = (bf16[192,2048]{1,0:T(8,128)(2,1)S(1)}, bf16[192,2048]{1,0:T(8,128)(2,1)S(1)}, u32[]{:S(2)}, u32[]{:S(2)}) collective-permute-start(bf16[192,2048]{1,0:T(8,128)(2,1)S(1)} %fusion.44), channel_id=1, source_target_pairs={{0,16},{2,18},{16,0},{18,2},{1,17},{3,19},{17,1},{19,3},{4,20},{6,... | collective-permute-start | bytes 2359304 | tf_op jit(solution)/shard_map/ppermute | solution.py:226
  33.7 33.5 %collective-permute-start.2 = (bf16[192,2048]{1,0:T(8,128)(2,1)S(1)}, bf16[192,2048]{1,0:T(8,128)(2,1)S(1)}, u32[]{:S(2)}, u32[]{:S(2)}) collective-permute-start(bf16[192,2048]{1,0:T(8,128)(2,1)S(1)} %fusion.44), channel_id=1, source_target_pairs={{0,18},{2,16},{16,2},{18,0},{1,19},{3,17},{17,3},{19,1},{4,22},{6,... | collective-permute-start | bytes 2359304 | tf_op jit(solution)/shard_map/ppermute | solution.py:226
  34.2 35.0 %copy-start.1 = (bf16[1,192,2048]{2,1,0:T(8,128)(2,1)}, bf16[1,192,2048]{2,1,0:T(8,128)(2,1)S(1)}, u32[]{:S(2)}) copy-start(bf16[1,192,2048]{2,1,0:T(8,128)(2,1)S(1)} %fusion.78) | copy-start | bytes 2359300
  50.0 19.2 %copy-start.6 = (bf16[192,2048]{1,0:T(8,128)(2,1)}, bf16[192,2048]{1,0:T(8,128)(2,1)S(1)}, u32[]{:S(2)}) copy-start(bf16[192,2048]{1,0:T(8,128)(2,1)S(1)} %collective-permute-done) | copy-start | bytes 2359300
  52.6 16.5 %copy-start.8 = (bf16[192,2048]{1,0:T(8,128)(2,1)}, bf16[192,2048]{1,0:T(8,128)(2,1)S(1)}, u32[]{:S(2)}) copy-start(bf16[192,2048]{1,0:T(8,128)(2,1)S(1)} %collective-permute-done.1) | copy-start | bytes 2359300
  69.2 55.1 %collective-permute-start.3 = (bf16[4,192,2048]{2,1,0:T(8,128)(2,1)}, bf16[4,192,2048]{2,1,0:T(8,128)(2,1)}, u32[]{:S(2)}, u32[]{:S(2)}) collective-permute-start(bf16[4,192,2048]{2,1,0:T(8,128)(2,1)} %pad_maximum_fusion.1), channel_id=1, source_target_pairs={{0,1},{1,0},{2,3},{3,2},{4,5},{5,4},{6,7},{7,6},{8,9},{9,8},{10,11... | collective-permute-start | bytes 9437192 | tf_op jit(solution)/shard_map/ppermute | solution.py:179
  69.3 51.1 %collective-permute-start.5 = (f32[384,1]{0,1:T(1,128)S(1)}, f32[384,1]{0,1:T(1,128)S(1)}, u32[]{:S(2)}, u32[]{:S(2)}) collective-permute-start(f32[384,1]{0,1:T(1,128)S(1)} %get-tuple-element.134), channel_id=1, source_target_pairs={{0,2},{2,0},{16,18},{18,16},{1,3},{3,1},{17,19},{19,17},{4,6},{6,4... | collective-permute-start | bytes 4616 | tf_op jit(solution)/shard_map/ppermute | solution.py:226
  70.9 49.6 %collective-permute-start.6 = (f32[384,1]{0,1:T(1,128)S(1)}, f32[384,1]{0,1:T(1,128)S(1)}, u32[]{:S(2)}, u32[]{:S(2)}) collective-permute-start(f32[384,1]{0,1:T(1,128)S(1)} %get-tuple-element.136), channel_id=1, source_target_pairs={{0,16},{2,18},{16,0},{18,2},{1,17},{3,19},{17,1},{19,3},{4,20},{6,... | collective-permute-start | bytes 4616 | tf_op jit(solution)/shard_map/ppermute | solution.py:226
  72.3 48.2 %collective-permute-start.7 = (f32[384,1]{0,1:T(1,128)S(1)}, f32[384,1]{0,1:T(1,128)S(1)}, u32[]{:S(2)}, u32[]{:S(2)}) collective-permute-start(f32[384,1]{0,1:T(1,128)S(1)} %get-tuple-element.135), channel_id=1, source_target_pairs={{0,18},{2,16},{16,2},{18,0},{1,19},{3,17},{17,3},{19,1},{4,22},{6,... | collective-permute-start | bytes 4616 | tf_op jit(solution)/shard_map/ppermute | solution.py:226
  75.7 45.0 %collective-permute-start.8 = (bf16[1280,256]{1,0:T(8,128)(2,1)S(1)}, bf16[1280,256]{1,0:T(8,128)(2,1)S(1)}, u32[]{:S(2)}, u32[]{:S(2)}) collective-permute-start(bf16[1280,256]{1,0:T(8,128)(2,1)S(1)} %pad_maximum_fusion.8), channel_id=1, source_target_pairs={{0,2},{2,0},{1,3},{3,1},{4,6},{6,4},{5,7},{7,5},{8,10},{10,8},{9,1... | collective-permute-start | bytes 1966088 | tf_op jit(solution)/shard_map/ppermute | solution.py:179
  124.2 213.5 %all-gather.8.cloned.1.call-start = ((), (), s32[]{:S(2)}) async-start(), calls=%async_computation.2 | async-start | bytes 5242880 | tf_op jit(solution)/shard_map/all_gather | solution.py:246
  238.1 5.7 %collective-permute-start.9 = (bf16[4,192,2048]{2,1,0:T(8,128)(2,1)S(1)}, bf16[4,192,2048]{2,1,0:T(8,128)(2,1)S(1)}, u32[]{:S(2)}, u32[]{:S(2)}) collective-permute-start(bf16[4,192,2048]{2,1,0:T(8,128)(2,1)S(1)} %constant_dynamic-slice_fusion.1), channel_id=1, source_target_pairs={{0,1},{1,0},{2,3},{3,2},{4,5},{5,4},{6,7},{7,6},{8,9},{9,8},{10,11... | collective-permute-start | bytes 9437192 | tf_op jit(solution)/shard_map/ppermute | solution.py:179
  239.5 14.9 %collective-permute-start.17 = (bf16[256,1024]{1,0:T(8,128)(2,1)S(1)}, bf16[256,1024]{1,0:T(8,128)(2,1)S(1)}, u32[]{:S(2)}, u32[]{:S(2)}) collective-permute-start(bf16[256,1024]{1,0:T(8,128)(2,1)S(1)} %dynamic-slice_convert_fusion), channel_id=1, source_target_pairs={{0,2},{2,0},{1,3},{3,1},{4,6},{6,4},{5,7},{7,5},{8,10},{10,8},{9,1... | collective-permute-start | bytes 1572872 | tf_op jit(solution)/shard_map/ppermute | solution.py:179
  249.8 37.9 %copy-start = (bf16[384,2048]{1,0:T(8,128)(2,1)S(1)}, bf16[384,2048]{1,0:T(8,128)(2,1)}, u32[]{:S(2)}) copy-start(bf16[384,2048]{1,0:T(8,128)(2,1)} %param.24) | copy-start | bytes 4718596
  249.8 22.0 %collective-permute-start.10 = (bf16[192,2048]{1,0:T(8,128)(2,1)}, bf16[192,2048]{1,0:T(8,128)(2,1)S(1)}, u32[]{:S(2)}, u32[]{:S(2)}) collective-permute-start(bf16[192,2048]{1,0:T(8,128)(2,1)} %get-tuple-element.110), channel_id=1, source_target_pairs={{0,2},{2,0},{16,18},{18,16},{1,3},{3,1},{17,19},{19,17},{4,6},{6,4... | collective-permute-start | bytes 2359304 | tf_op jit(solution)/shard_map/ppermute | solution.py:226
  251.4 20.6 %collective-permute-start.11 = (bf16[192,2048]{1,0:T(8,128)(2,1)}, bf16[192,2048]{1,0:T(8,128)(2,1)S(1)}, u32[]{:S(2)}, u32[]{:S(2)}) collective-permute-start(bf16[192,2048]{1,0:T(8,128)(2,1)} %get-tuple-element.112), channel_id=1, source_target_pairs={{0,16},{2,18},{16,0},{18,2},{1,17},{3,19},{17,1},{19,3},{4,20},{6,... | collective-permute-start | bytes 2359304 | tf_op jit(solution)/shard_map/ppermute | solution.py:226
  252.9 34.8 %collective-permute-start.12 = (bf16[192,2048]{1,0:T(8,128)(2,1)}, bf16[192,2048]{1,0:T(8,128)(2,1)}, u32[]{:S(2)}, u32[]{:S(2)}) collective-permute-start(bf16[192,2048]{1,0:T(8,128)(2,1)} %get-tuple-element.111), channel_id=1, source_target_pairs={{0,18},{2,16},{16,2},{18,0},{1,19},{3,17},{17,3},{19,1},{4,22},{6,... | collective-permute-start | bytes 2359304 | tf_op jit(solution)/shard_map/ppermute | solution.py:226
  256.8 33.5 %copy-start.14 = (f32[2048]{0:T(1024)S(1)}, f32[2048]{0:T(1024)}, u32[]{:S(2)}) copy-start(f32[2048]{0:T(1024)} %param.41) | copy-start | bytes 24580
  272.0 15.7 %copy-start.11 = (bf16[192,2048]{1,0:T(8,128)(2,1)}, bf16[192,2048]{1,0:T(8,128)(2,1)S(1)}, u32[]{:S(2)}) copy-start(bf16[192,2048]{1,0:T(8,128)(2,1)S(1)} %collective-permute-done.11) | copy-start | bytes 2359300
  290.6 19.6 %collective-permute-start.13 = (bf16[192,2048]{1,0:T(8,128)(2,1)S(1)}, bf16[192,2048]{1,0:T(8,128)(2,1)S(1)}, u32[]{:S(2)}, u32[]{:S(2)}) collective-permute-start(bf16[192,2048]{1,0:T(8,128)(2,1)S(1)} %fusion.33), channel_id=1, source_target_pairs={{0,2},{2,0},{16,18},{18,16},{1,3},{3,1},{17,19},{19,17},{4,6},{6,4... | collective-permute-start | bytes 2359304 | tf_op jit(solution)/shard_map/ppermute | solution.py:226
  292.3 20.4 %collective-permute-start.14 = (bf16[192,2048]{1,0:T(8,128)(2,1)S(1)}, bf16[192,2048]{1,0:T(8,128)(2,1)S(1)}, u32[]{:S(2)}, u32[]{:S(2)}) collective-permute-start(bf16[192,2048]{1,0:T(8,128)(2,1)S(1)} %fusion.33), channel_id=1, source_target_pairs={{0,16},{2,18},{16,0},{18,2},{1,17},{3,19},{17,1},{19,3},{4,20},{6,... | collective-permute-start | bytes 2359304 | tf_op jit(solution)/shard_map/ppermute | solution.py:226
  293.7 33.4 %collective-permute-start.15 = (bf16[192,2048]{1,0:T(8,128)(2,1)S(1)}, bf16[192,2048]{1,0:T(8,128)(2,1)S(1)}, u32[]{:S(2)}, u32[]{:S(2)}) collective-permute-start(bf16[192,2048]{1,0:T(8,128)(2,1)S(1)} %fusion.33), channel_id=1, source_target_pairs={{0,18},{2,16},{16,2},{18,0},{1,19},{3,17},{17,3},{19,1},{4,22},{6,... | collective-permute-start | bytes 2359304 | tf_op jit(solution)/shard_map/ppermute | solution.py:226
  327.5 5.7 %collective-permute-start.16 = (bf16[4,192,2048]{2,1,0:T(8,128)(2,1)S(1)}, bf16[4,192,2048]{2,1,0:T(8,128)(2,1)S(1)}, u32[]{:S(2)}, u32[]{:S(2)}) collective-permute-start(bf16[4,192,2048]{2,1,0:T(8,128)(2,1)S(1)} %pad_maximum_fusion.2), channel_id=1, source_target_pairs={{0,1},{1,0},{2,3},{3,2},{4,5},{5,4},{6,7},{7,6},{8,9},{9,8},{10,11... | collective-permute-start | bytes 9437192 | tf_op jit(solution)/shard_map/ppermute | solution.py:179
  359.8 5.7 %collective-permute-start.18 = (bf16[4,192,2048]{2,1,0:T(8,128)(2,1)S(1)}, bf16[4,192,2048]{2,1,0:T(8,128)(2,1)S(1)}, u32[]{:S(2)}, u32[]{:S(2)}) collective-permute-start(bf16[4,192,2048]{2,1,0:T(8,128)(2,1)S(1)} %constant_dynamic-slice_fusion), channel_id=1, source_target_pairs={{0,1},{1,0},{2,3},{3,2},{4,5},{5,4},{6,7},{7,6},{8,9},{9,8},{10,11... | collective-permute-start | bytes 9437192 | tf_op jit(solution)/shard_map/ppermute | solution.py:179
  367.5 19.6 %collective-permute-start.19 = (bf16[192,2048]{1,0:T(8,128)(2,1)S(1)}, bf16[192,2048]{1,0:T(8,128)(2,1)S(1)}, u32[]{:S(2)}, u32[]{:S(2)}) collective-permute-start(bf16[192,2048]{1,0:T(8,128)(2,1)S(1)} %get-tuple-element.107), channel_id=1, source_target_pairs={{0,2},{2,0},{16,18},{18,16},{1,3},{3,1},{17,19},{19,17},{4,6},{6,4... | collective-permute-start | bytes 2359304 | tf_op jit(solution)/shard_map/ppermute | solution.py:226
  369.2 20.4 %collective-permute-start.20 = (bf16[192,2048]{1,0:T(8,128)(2,1)S(1)}, bf16[192,2048]{1,0:T(8,128)(2,1)S(1)}, u32[]{:S(2)}, u32[]{:S(2)}) collective-permute-start(bf16[192,2048]{1,0:T(8,128)(2,1)S(1)} %get-tuple-element.109), channel_id=1, source_target_pairs={{0,16},{2,18},{16,0},{18,2},{1,17},{3,19},{17,1},{19,3},{4,20},{6,... | collective-permute-start | bytes 2359304 | tf_op jit(solution)/shard_map/ppermute | solution.py:226
  370.7 34.5 %collective-permute-start.21 = (bf16[192,2048]{1,0:T(8,128)(2,1)S(1)}, bf16[192,2048]{1,0:T(8,128)(2,1)S(1)}, u32[]{:S(2)}, u32[]{:S(2)}) collective-permute-start(bf16[192,2048]{1,0:T(8,128)(2,1)S(1)} %get-tuple-element.108), channel_id=1, source_target_pairs={{0,18},{2,16},{16,2},{18,0},{1,19},{3,17},{17,3},{19,1},{4,22},{6,... | collective-permute-start | bytes 2359304 | tf_op jit(solution)/shard_map/ppermute | solution.py:226
  405.8 2.4 collective-permute-start.22
  (18 other events, 58.8 us)
Sparse Core Ops, SparseCore 0:
  26.6 73.5 all-gather.3
  124.4 97.5 all-gather.5
  257.0 79.8 all-gather.7
